TPU v7x, 32 devices: a whole 2x2x4 slice. The times are simulated.
32 devices in a mesh: ra: 4 (over z), cb: 4 (over y, x), dp: 2 (over core).
Axes of the slice: x: 2, y: 2, z: 4, core: 2. Of those that a mesh axis runs over, the one named last changes fastest.
Arguments:
- stream: bfloat16 [3072, 4096], P(('cb', 'dp'), 'ra'), may hold values from -20 to 20
- up_first: bfloat16 [4096, 16384], P('cb', 'ra'), may hold values from -0.09375 to 0.09375
- down_first: bfloat16 [16384, 4096], P('ra', 'cb'), may hold values from -0.046875 to 0.046875
- up_second: bfloat16 [4096, 16384], P('cb', 'ra'), may hold values from -0.09375 to 0.09375
- down_second: bfloat16 [16384, 4096], P('ra', 'cb'), may hold values from -0.046875 to 0.046875
- gain_first: float32 [4096], P('ra'), may hold values from 0.1 to 1.9
- bias_first: float32 [4096], P('ra'), may hold values from -3 to 3
- gain_second: float32 [4096], P('ra'), may hold values from 0.1 to 1.9
- bias_second: float32 [4096], P('ra'), may hold values from -3 to 3
Outputs:
- result: bfloat16 [3072, 4096], P(('cb', 'dp'), 'ra')
All inputs are finite; a program needn't handle non-finite values.
Results may differ from a plain program's by a relative error of at most 0.0093.
Values may be sent and summed in bfloat16 or wider, within the bound.
A program may use at most 192 MiB of HBM per device.

v0:
```python
import jax
import jax.numpy as jnp
from jax import lax
from jax.sharding import PartitionSpec as P

RESID = 1.4142135
EPS = 0.5


def sublayer(x, up, down, gain, bias):
    whole = lax.all_gather(x, "ra", axis=1, tiled=True)
    pre = jnp.dot(
        whole, lax.all_gather(up, "cb", axis=0, tiled=True), preferred_element_type=jnp.float32
    )
    hidden = jnp.square(jax.nn.relu(pre)).astype(jnp.bfloat16)
    partial_sums = jnp.dot(
        hidden, lax.all_gather(down, "cb", axis=1, tiled=True), preferred_element_type=jnp.float32
    )
    branch = lax.psum_scatter(partial_sums, "ra", scatter_dimension=1, tiled=True)
    mixed = RESID * x.astype(jnp.float32) + branch
    width = mixed.shape[1] * lax.axis_size("ra")
    total, squares = lax.psum(
        (jnp.sum(mixed, axis=1, keepdims=True), jnp.sum(mixed * mixed, axis=1, keepdims=True)), "ra"
    )
    mean = total / width
    var = squares / width - mean * mean
    centered = mixed - mean
    return (centered * lax.rsqrt(var + EPS) * gain + bias).astype(jnp.bfloat16)


def body(
    stream,
    up_first,
    down_first,
    up_second,
    down_second,
    gain_first,
    bias_first,
    gain_second,
    bias_second,
):
    x = stream
    for up, down, gain, bias in (
        (up_first, down_first, gain_first, bias_first),
        (up_second, down_second, gain_second, bias_second),
    ):
        x = sublayer(x, up, down, gain, bias)
    return x


def solution(mesh):
    placed = (
        P(("cb", "dp"), "ra"),
        P("cb", "ra"),
        P("ra", "cb"),
        P("cb", "ra"),
        P("ra", "cb"),
        P("ra"),
        P("ra"),
        P("ra"),
        P("ra"),
    )
    return jax.shard_map(
        body, mesh=mesh, in_specs=placed, out_specs=P(("cb", "dp"), "ra"), check_vma=False
    )
```

profile of v0, /device:TPU:0, one launch (start us, length us, event | category | flops | bytes accessed | tf_op | source)
XLA Modules:
  0.0 1616.1 jit_solution(16480345639922610143)
XLA Ops:
  6.5 0.7 all-gather.7.cloned.1.call-update
  7.3 0.7 all-gather.9.cloned.1.call-update
  8.1 0.7 all-gather.11.cloned.1.call-update
  8.8 66.3 %all-gather.7.cloned.1.call-done = bf16[384,4096]{1,0:T(8,128)(2,1)} async-done(((bf16[384,1024]{1,0:T(8,128)(2,1)}), bf16[384,4096]{1,0:T(8,128)(2,1)}) %all-gather.7.cloned.1.call-update) | async-done | bytes 3145744 | tf_op jit(solution)/shard_map/all_gather | solution.py:11
  75.1 297.6 %all-gather.9.cloned.1.call-done = bf16[4096,4096]{1,0:T(8,128)(2,1)} async-done(((bf16[1024,4096]{1,0:T(8,128)(2,1)}), bf16[4096,4096]{1,0:T(8,128)(2,1)}) %all-gather.9.cloned.1.call-update) | async-done | bytes 33554448 | tf_op jit(solution)/shard_map/all_gather | solution.py:13
  372.7 21.7 %fusion.37 = bf16[384,4096]{1,0:T(8,128)(2,1)S(1)} fusion(bf16[4096,4096]{1,0:T(8,128)(2,1)} %all-gather.9.cloned.1.call-done, bf16[384,4096]{1,0:T(8,128)(2,1)} %all-gather.7.cloned.1.call-done), kind=kOutput, calls=%bitcast_fusion.2.clone.1 | convolution fusion | flops 12889620480 | bytes 39845888 | tf_op jit(solution)/shard_map/dot_general | solution.py:12
  394.4 277.2 %all-gather.11.cloned.1.call-done = bf16[4096,4096]{1,0:T(8,128)(2,1)} async-done(((bf16[4096,1024]{1,0:T(8,128)(2,1)}), bf16[4096,4096]{1,0:T(8,128)(2,1)}) %all-gather.11.cloned.1.call-update) | async-done | bytes 33554448 | tf_op jit(solution)/shard_map/all_gather | solution.py:17
  671.7 19.7 %fusion.2 = f32[384,4096]{1,0:T(8,128)} fusion(bf16[4096,4096]{1,0:T(8,128)(2,1)} %all-gather.11.cloned.1.call-done, bf16[384,4096]{1,0:T(8,128)(2,1)S(1)} %fusion.37), kind=kOutput, calls=%fused_computation.14 | convolution fusion | flops 12884901888 | bytes 42991616 | tf_op jit(solution)/shard_map/dot_general | solution.py:16
  691.5 0.5 all-gather.15.cloned.1.call-update
  692.1 110.3 %reduce-scatter.3.cloned.1.call-done = f32[384,1024]{1,0:T(8,128)} async-done(((f32[384,4096]{1,0:T(8,128)}), f32[384,1024]{1,0:T(8,128)}) %reduce-scatter.3.cloned.1.call-update) | async-done | bytes 1572880 | tf_op jit(solution)/shard_map/reduce_scatter | solution.py:19
  802.3 1.9 fusion
  804.3 11.0 all-reduce.1
  815.3 1.3 add_convert_fusion.1
  816.7 0.7 all-gather.17.cloned.1.call-update
  817.4 0.2 reduce-scatter.5.cloned.1.call-start
  817.7 284.0 %all-gather.15.cloned.1.call-done = bf16[4096,4096]{1,0:T(8,128)(2,1)} async-done(((bf16[1024,4096]{1,0:T(8,128)(2,1)}), bf16[4096,4096]{1,0:T(8,128)(2,1)}) %all-gather.15.cloned.1.call-update) | async-done | bytes 33554448 | tf_op jit(solution)/shard_map/all_gather | solution.py:13
  1101.7 64.9 %all-gather.13.cloned.1.call-done = bf16[384,4096]{1,0:T(8,128)(2,1)} async-done(((bf16[384,1024]{1,0:T(8,128)(2,1)}), bf16[384,4096]{1,0:T(8,128)(2,1)}) %all-gather.13.cloned.1.call-update) | async-done | bytes 3145744 | tf_op jit(solution)/shard_map/all_gather | solution.py:11
  1166.6 22.8 %fusion.41 = bf16[384,4096]{1,0:T(8,128)(2,1)S(1)} fusion(bf16[4096,4096]{1,0:T(8,128)(2,1)} %all-gather.15.cloned.1.call-done, bf16[384,4096]{1,0:T(8,128)(2,1)} %all-gather.13.cloned.1.call-done), kind=kOutput, calls=%bitcast_fusion.3.clone | convolution fusion | flops 12889620480 | bytes 39845888 | tf_op jit(solution)/shard_map/dot_general | solution.py:12
  1189.4 274.8 %all-gather.17.cloned.1.call-done = bf16[4096,4096]{1,0:T(8,128)(2,1)} async-done(((bf16[4096,1024]{1,0:T(8,128)(2,1)}), bf16[4096,4096]{1,0:T(8,128)(2,1)}) %all-gather.17.cloned.1.call-update) | async-done | bytes 33554448 | tf_op jit(solution)/shard_map/all_gather | solution.py:17
  1464.2 19.8 %fusion.3 = f32[384,4096]{1,0:T(8,128)} fusion(bf16[4096,4096]{1,0:T(8,128)(2,1)} %all-gather.17.cloned.1.call-done, bf16[384,4096]{1,0:T(8,128)(2,1)S(1)} %fusion.41), kind=kOutput, calls=%fused_computation.15 | convolution fusion | flops 12884901888 | bytes 42991616 | tf_op jit(solution)/shard_map/dot_general | solution.py:16
  1484.0 110.9 %reduce-scatter.5.cloned.1.call-done = f32[384,1024]{1,0:T(8,128)} async-done(((f32[384,4096]{1,0:T(8,128)}), f32[384,1024]{1,0:T(8,128)}) %reduce-scatter.5.cloned.1.call-update) | async-done | bytes 1572880 | tf_op jit(solution)/shard_map/reduce_scatter | solution.py:19
  1594.9 1.9 fusion.1
  1596.9 11.0 all-reduce
  1607.9 1.3 add_convert_fusion
  (32 shorter events, 0.4 us)
Async XLA Ops:
  6.5 68.6 %all-gather.7.cloned.1.call-start = ((), (), s32[]{:S(2)}) async-start(), calls=%async_computation.2 | async-start | bytes 3932160 | tf_op jit(solution)/shard_map/all_gather | solution.py:11
  7.3 365.4 %all-gather.9.cloned.1.call-start = ((), (), s32[]{:S(2)}) async-start(), calls=%async_computation.3 | async-start | bytes 41943040 | tf_op jit(solution)/shard_map/all_gather | solution.py:13
  8.0 663.7 %all-gather.11.cloned.1.call-start = ((), (), s32[]{:S(2)}) async-start(), calls=%async_computation.4 | async-start | bytes 41943040 | tf_op jit(solution)/shard_map/all_gather | solution.py:17
  8.7 793.6 %reduce-scatter.3.cloned.1.call-start = ((), (), s32[]{:S(2)}) async-start(), calls=%async_computation.5 | async-start | bytes 7864320 | tf_op jit(solution)/shard_map/reduce_scatter | solution.py:19
  691.4 110.9 %copy-start.1 = (bf16[384,1024]{1,0:T(8,128)(2,1)S(1)}, bf16[384,1024]{1,0:T(8,128)(2,1)}, u32[]{:S(2)}) copy-start(bf16[384,1024]{1,0:T(8,128)(2,1)} %param.9) | copy-start | bytes 2359300
  691.4 123.9 %copy-start.4 = (f32[1024]{0:T(1024)S(1)}, f32[1024]{0:T(1024)}, u32[]{:S(2)}) copy-start(f32[1024]{0:T(1024)} %param.15) | copy-start | bytes 12292
  691.4 123.9 %copy-start.5 = (f32[1024]{0:T(1024)S(1)}, f32[1024]{0:T(1024)}, u32[]{:S(2)}) copy-start(f32[1024]{0:T(1024)} %param.14) | copy-start | bytes 12292
  691.4 410.2 %all-gather.15.cloned.1.call-start = ((), (), s32[]{:S(2)}) async-start(), calls=%async_computation.7 | async-start | bytes 41943040 | tf_op jit(solution)/shard_map/all_gather | solution.py:13
  692.0 474.5 %all-gather.13.cloned.1.call-start = ((), (), s32[]{:S(2)}) async-start(), calls=%async_computation.6 | async-start | bytes 3932160 | tf_op jit(solution)/shard_map/all_gather | solution.py:11
  802.3 13.0 copy-start.2
  816.7 647.5 %all-gather.17.cloned.1.call-start = ((), (), s32[]{:S(2)}) async-start(), calls=%async_computation.8 | async-start | bytes 41943040 | tf_op jit(solution)/shard_map/all_gather | solution.py:17
  817.4 777.5 %reduce-scatter.5.cloned.1.call-start = ((), (), s32[]{:S(2)}) async-start(), calls=%async_computation.9 | async-start | bytes 7864320 | tf_op jit(solution)/shard_map/reduce_scatter | solution.py:19
  1483.9 111.0 %copy-start = (bf16[384,1024]{1,0:T(8,128)(2,1)S(1)}, bf16[384,1024]{1,0:T(8,128)(2,1)}, u32[]{:S(2)}) copy-start(bf16[384,1024]{1,0:T(8,128)(2,1)} %add_convert_fusion.1) | copy-start | bytes 2359300
  1483.9 123.9 %copy-start.6 = (f32[1024]{0:T(1024)S(1)}, f32[1024]{0:T(1024)}, u32[]{:S(2)}) copy-start(f32[1024]{0:T(1024)} %param.17) | copy-start | bytes 12292
  1483.9 123.9 %copy-start.7 = (f32[1024]{0:T(1024)S(1)}, f32[1024]{0:T(1024)}, u32[]{:S(2)}) copy-start(f32[1024]{0:T(1024)} %param.16) | copy-start | bytes 12292
  1594.9 13.0 copy-start.3
Sparse Core Ops, SparseCore 0:
  8.9 66.1 all-gather.6
  76.9 295.7 all-gather.8
  374.6 297.0 all-gather.10
  691.5 110.7 reduce-scatter.2
  804.0 297.5 all-gather.14
  1103.1 63.4 all-gather.12
  1168.4 295.7 all-gather.16
  1484.1 110.7 reduce-scatter.4
where the time goes:
time: 1620 us
  waiting for transfers between devices  1490 us (92%)
  matrix products  84 us (5%)
  blocking collectives  21.9 us (1%)
    all_gather x2, waiting for transfers between devices, sublayer(): lax.all_gather(up, 'cb', axis=0, tiled=True)  582 us
    all_gather x2, waiting for transfers between devices, sublayer(): lax.all_gather(down, 'cb', axis=1, tiled=True)  552 us
    reduce_scatter x2, waiting for transfers between devices, sublayer(): lax.psum_scatter(partial_sums, 'ra', scatter_dimension=1, tiled=True)  221 us
    all_gather x2, waiting for transfers between devices, sublayer(): whole = lax.all_gather(x, 'ra', axis=1, tiled=True)  131 us
    dot_general x2, matrix products, sublayer(): jnp.dot(whole, lax.all_gather(up, 'cb', axis=0, tiled=True), preferred_el...  44.5 us
    dot_general x2, matrix products, sublayer(): jnp.dot(hidden, lax.all_gather(down, 'cb', axis=1, tiled=True), preferred...  39.5 us
  transfers between devices with their start and end apart: 8, of which 8 were waited for; matrix products, arithmetic and copies ran while one was open for 3% of the time, Pallas kernels for 0%

commit v1 on v0

--- a/solution.py
+++ b/solution.py
@@ -7,8 +7,19 @@
 EPS = 0.5
 
 
+def gather_by_hops(x, mesh_axis, d):
+    size = lax.axis_size(mesh_axis)
+    right = [(i, (i + 1) % size) for i in range(size)]
+    pieces = [x]
+    for far in range(1, size):
+        pieces = [lax.ppermute(pieces[0], mesh_axis, right), *pieces]
+    whole = jnp.concatenate(pieces, axis=d)
+    shift = (lax.axis_index(mesh_axis) + 1) * pieces[-1].shape[d]
+    return jnp.roll(whole, shift, axis=d)
+
+
 def sublayer(x, up, down, gain, bias):
-    whole = lax.all_gather(x, "ra", axis=1, tiled=True)
+    whole = gather_by_hops(x, "ra", 1)
     pre = jnp.dot(
         whole, lax.all_gather(up, "cb", axis=0, tiled=True), preferred_element_type=jnp.float32
     )

time: 1620 us -> 1490 us (0.920)
  waiting for transfers between devices: 1490 us -> 1350 us
    all_gather x2 -> x0, waiting for transfers between devices: 131 us -> none  [sublayer(): whole = lax.all_gather(x, 'ra', axis=1, tiled=True)]
    ppermute x0 -> x6, waiting for transfers between devices: none -> 97.6 us  [gather_by_hops(): pieces = [lax.ppermute(pieces[0], mesh_axis, right), *pieces]]
    all_gather x2, waiting for transfers between devices: 582 us -> 484 us  [sublayer(): lax.all_gather(up, 'cb', axis=0, tiled=True)]
  transfers between devices with their start and end apart: 8 -> 12, of which waited for: 8 -> 11; matrix products, arithmetic and copies ran while one was open for 3% -> 4% of each run, Pallas kernels for 0% -> 0%
where the time goes in v1:
time: 1490 us
  waiting for transfers between devices  1350 us (91%)
  matrix products  99.5 us (7%)
  blocking collectives  21.9 us (1%)
    all_gather x2, waiting for transfers between devices, sublayer(): lax.all_gather(down, 'cb', axis=1, tiled=True)  542 us
    all_gather x2, waiting for transfers between devices, sublayer(): lax.all_gather(up, 'cb', axis=0, tiled=True)  484 us
    reduce_scatter x2, waiting for transfers between devices, sublayer(): lax.psum_scatter(partial_sums, 'ra', scatter_dimension=1, tiled=True)  221 us
    ppermute x6, waiting for transfers between devices, gather_by_hops(): pieces = [lax.ppermute(pieces[0], mesh_axis, right), *pieces]  97.6 us
    dot_general x2, matrix products, sublayer(): jnp.dot(whole, lax.all_gather(up, 'cb', axis=0, tiled=True), preferred_el...  56.3 us
    dot_general x2, matrix products, sublayer(): jnp.dot(hidden, lax.all_gather(down, 'cb', axis=1, tiled=True), preferred...  43.2 us
  transfers between devices with their start and end apart: 12, of which 11 were waited for; matrix products, arithmetic and copies ran while one was open for 4% of the time, Pallas kernels for 0%

profile of v1, /device:TPU:0, one launch (start us, length us, event | category | flops | bytes accessed | tf_op | source)
XLA Modules:
  0.0 1493.7 jit_solution(16241074446072122666)
XLA Ops:
  6.5 0.7 all-gather.5.cloned.1.call-update
  7.3 0.7 all-gather.7.cloned.1.call-update
  8.1 3.1 collective-permute-start
  11.2 19.6 %collective-permute-done = bf16[384,1024]{1,0:T(8,128)(2,1)S(1)} collective-permute-done((bf16[384,1024]{1,0:T(8,128)(2,1)S(1)}, bf16[384,1024]{1,0:T(8,128)(2,1)S(1)}, u32[]{:S(2)}, u32[]{:S(2)}) %collective-permute-start) | collective-permute-done | bytes 786464 | tf_op jit(solution)/shard_map/ppermute | solution.py:15
  30.7 20.5 %collective-permute-done.1 = bf16[384,1024]{1,0:T(8,128)(2,1)S(1)} collective-permute-done((bf16[384,1024]{1,0:T(8,128)(2,1)S(1)}, bf16[384,1024]{1,0:T(8,128)(2,1)S(1)}, u32[]{:S(2)}, u32[]{:S(2)}) %collective-permute-start.1) | collective-permute-done | bytes 786464 | tf_op jit(solution)/shard_map/ppermute | solution.py:15
  51.2 19.6 %collective-permute-done.2 = bf16[384,1024]{1,0:T(8,128)(2,1)S(1)} collective-permute-done((bf16[384,1024]{1,0:T(8,128)(2,1)S(1)}, bf16[384,1024]{1,0:T(8,128)(2,1)S(1)}, u32[]{:S(2)}, u32[]{:S(2)}) %collective-permute-start.2) | collective-permute-done | bytes 786464 | tf_op jit(solution)/shard_map/ppermute | solution.py:15
  70.9 238.1 %all-gather.5.cloned.1.call-done = bf16[4096,4096]{1,0:T(8,128)(2,1)} async-done(((bf16[1024,4096]{1,0:T(8,128)(2,1)}), bf16[4096,4096]{1,0:T(8,128)(2,1)}) %all-gather.5.cloned.1.call-update) | async-done | bytes 33554448 | tf_op jit(solution)/shard_map/all_gather | solution.py:24
  309.0 28.1 %multiply_convert_fusion.1 = bf16[384,4096]{1,0:T(8,128)(2,1)} fusion(bf16[4096,4096]{1,0:T(8,128)(2,1)} %all-gather.5.cloned.1.call-done, s32[]{:T(128)S(6)} %select_n.13, bf16[384,1024]{1,0:T(8,128)(2,1)S(1)} %collective-permute-done.2, bf16[384,1024]{1,0:T(8,128)(2,1)S(1)} %collective-permute-done.1, bf16[384,1024]{1,0:T(8,128)(2,1)S(1)} %collective-permute-done, ...), kind=kOutput, calls=%fused_computation.17 | convolution fusion | flops 12914786304 | bytes 39845892 | tf_op jit(solution)/shard_map/dot_general | solution.py:23
  337.1 270.8 %all-gather.7.cloned.1.call-done = bf16[4096,4096]{1,0:T(8,128)(2,1)} async-done(((bf16[4096,1024]{1,0:T(8,128)(2,1)}), bf16[4096,4096]{1,0:T(8,128)(2,1)}) %all-gather.7.cloned.1.call-update) | async-done | bytes 33554448 | tf_op jit(solution)/shard_map/all_gather | solution.py:28
  608.0 21.7 %fusion.24 = f32[384,4096]{1,0:T(8,128)} fusion(bf16[384,4096]{1,0:T(8,128)(2,1)} %multiply_convert_fusion.1, bf16[4096,4096]{1,0:T(8,128)(2,1)} %all-gather.7.cloned.1.call-done), kind=kOutput, calls=%fused_computation.48 | convolution fusion | flops 12884901888 | bytes 42991616 | tf_op jit(solution)/shard_map/dot_general | solution.py:27
  630.9 109.7 %reduce-scatter.3.cloned.1.call-done = f32[384,1024]{1,0:T(8,128)} async-done(((f32[384,4096]{1,0:T(8,128)}), f32[384,1024]{1,0:T(8,128)}) %reduce-scatter.3.cloned.1.call-update) | async-done | bytes 1572880 | tf_op jit(solution)/shard_map/reduce_scatter | solution.py:30
  740.6 1.8 fusion.18
  742.5 11.0 all-reduce.1
  753.5 2.4 add_convert_fusion.1
  756.0 19.3 %collective-permute-done.3 = bf16[384,1024]{1,0:T(8,128)(2,1)S(1)} collective-permute-done((bf16[384,1024]{1,0:T(8,128)(2,1)S(1)}, bf16[384,1024]{1,0:T(8,128)(2,1)S(1)}, u32[]{:S(2)}, u32[]{:S(2)}) %collective-permute-start.3) | collective-permute-done | bytes 786464 | tf_op jit(solution)/shard_map/ppermute | solution.py:15
  775.3 18.5 %collective-permute-done.4 = bf16[384,1024]{1,0:T(8,128)(2,1)S(1)} collective-permute-done((bf16[384,1024]{1,0:T(8,128)(2,1)S(1)}, bf16[384,1024]{1,0:T(8,128)(2,1)S(1)}, u32[]{:S(2)}, u32[]{:S(2)}) %collective-permute-start.4) | collective-permute-done | bytes 786464 | tf_op jit(solution)/shard_map/ppermute | solution.py:15
  793.8 246.1 %all-gather.9.cloned.1.call-done = bf16[4096,4096]{1,0:T(8,128)(2,1)} async-done(((bf16[1024,4096]{1,0:T(8,128)(2,1)}), bf16[4096,4096]{1,0:T(8,128)(2,1)}) %all-gather.9.cloned.1.call-update) | async-done | bytes 33554448 | tf_op jit(solution)/shard_map/all_gather | solution.py:24
  1040.0 28.1 %multiply_convert_fusion = bf16[384,4096]{1,0:T(8,128)(2,1)} fusion(bf16[4096,4096]{1,0:T(8,128)(2,1)} %all-gather.9.cloned.1.call-done, s32[]{:T(128)S(6)} %select_n.13, bf16[384,1024]{1,0:T(8,128)(2,1)S(1)} %collective-permute-done.5, bf16[384,1024]{1,0:T(8,128)(2,1)S(1)} %collective-permute-done.4, bf16[384,1024]{1,0:T(8,128)(2,1)S(1)} %collective-permute-done.3, ...), kind=kOutput, calls=%fused_computation.16 | convolution fusion | flops 12914786304 | bytes 39845892 | tf_op jit(solution)/shard_map/dot_general | solution.py:23
  1068.1 270.7 %all-gather.11.cloned.1.call-done = bf16[4096,4096]{1,0:T(8,128)(2,1)} async-done(((bf16[4096,1024]{1,0:T(8,128)(2,1)}), bf16[4096,4096]{1,0:T(8,128)(2,1)}) %all-gather.11.cloned.1.call-update) | async-done | bytes 33554448 | tf_op jit(solution)/shard_map/all_gather | solution.py:28
  1338.8 21.6 %fusion.25 = f32[384,4096]{1,0:T(8,128)} fusion(bf16[384,4096]{1,0:T(8,128)(2,1)} %multiply_convert_fusion, bf16[4096,4096]{1,0:T(8,128)(2,1)} %all-gather.11.cloned.1.call-done), kind=kOutput, calls=%fused_computation.49 | convolution fusion | flops 12884901888 | bytes 42991616 | tf_op jit(solution)/shard_map/dot_general | solution.py:27
  1360.4 110.9 %reduce-scatter.5.cloned.1.call-done = f32[384,1024]{1,0:T(8,128)} async-done(((f32[384,4096]{1,0:T(8,128)}), f32[384,1024]{1,0:T(8,128)}) %reduce-scatter.5.cloned.1.call-update) | async-done | bytes 1572880 | tf_op jit(solution)/shard_map/reduce_scatter | solution.py:30
  1471.3 1.8 fusion.19
  1473.1 11.0 all-reduce
  1484.2 2.7 add_convert_fusion
  (32 shorter events, 1.5 us)
Async XLA Ops:
  6.5 1.5 copy-start
  6.5 302.5 %all-gather.5.cloned.1.call-start = ((), (), s32[]{:S(2)}) async-start(), calls=%async_computation.2 | async-start | bytes 41943040 | tf_op jit(solution)/shard_map/all_gather | solution.py:24
  7.3 600.7 %all-gather.7.cloned.1.call-start = ((), (), s32[]{:S(2)}) async-start(), calls=%async_computation.3 | async-start | bytes 41943040 | tf_op jit(solution)/shard_map/all_gather | solution.py:28
  8.0 732.6 %reduce-scatter.3.cloned.1.call-start = ((), (), s32[]{:S(2)}) async-start(), calls=%async_computation.4 | async-start | bytes 7864320 | tf_op jit(solution)/shard_map/reduce_scatter | solution.py:30
  8.1 22.7 %collective-permute-start = (bf16[384,1024]{1,0:T(8,128)(2,1)S(1)}, bf16[384,1024]{1,0:T(8,128)(2,1)S(1)}, u32[]{:S(2)}, u32[]{:S(2)}) collective-permute-start(bf16[384,1024]{1,0:T(8,128)(2,1)S(1)} %copy-done), channel_id=1, source_target_pairs={{0,8},{8,16},{16,24},{24,0},{1,9},{9,17},{17,25},{25,1},{2,10},{10... | collective-permute-start | bytes 2359304 | tf_op jit(solution)/shard_map/ppermute | solution.py:15
  30.7 20.5 %collective-permute-start.1 = (bf16[384,1024]{1,0:T(8,128)(2,1)S(1)}, bf16[384,1024]{1,0:T(8,128)(2,1)S(1)}, u32[]{:S(2)}, u32[]{:S(2)}) collective-permute-start(bf16[384,1024]{1,0:T(8,128)(2,1)S(1)} %collective-permute-done), channel_id=1, source_target_pairs={{0,8},{8,16},{16,24},{24,0},{1,9},{9,17},{17,25},{25,1},{2,10},{10... | collective-permute-start | bytes 2359304 | tf_op jit(solution)/shard_map/ppermute | solution.py:15
  51.2 19.6 %collective-permute-start.2 = (bf16[384,1024]{1,0:T(8,128)(2,1)S(1)}, bf16[384,1024]{1,0:T(8,128)(2,1)S(1)}, u32[]{:S(2)}, u32[]{:S(2)}) collective-permute-start(bf16[384,1024]{1,0:T(8,128)(2,1)S(1)} %collective-permute-done.1), channel_id=1, source_target_pairs={{0,8},{8,16},{16,24},{24,0},{1,9},{9,17},{17,25},{25,1},{2,10},{10... | collective-permute-start | bytes 2359304 | tf_op jit(solution)/shard_map/ppermute | solution.py:15
  629.7 410.3 %all-gather.9.cloned.1.call-start = ((), (), s32[]{:S(2)}) async-start(), calls=%async_computation.5 | async-start | bytes 41943040 | tf_op jit(solution)/shard_map/all_gather | solution.py:24
  630.3 123.2 %copy-start.1 = (f32[1024]{0:T(1024)S(1)}, f32[1024]{0:T(1024)}, u32[]{:S(2)}) copy-start(f32[1024]{0:T(1024)} %param.17) | copy-start | bytes 12292
  630.3 123.2 %copy-start.2 = (f32[1024]{0:T(1024)S(1)}, f32[1024]{0:T(1024)}, u32[]{:S(2)}) copy-start(f32[1024]{0:T(1024)} %param.16) | copy-start | bytes 12292
  630.3 708.5 %all-gather.11.cloned.1.call-start = ((), (), s32[]{:S(2)}) async-start(), calls=%async_computation.6 | async-start | bytes 41943040 | tf_op jit(solution)/shard_map/all_gather | solution.py:28
  630.9 840.4 %reduce-scatter.5.cloned.1.call-start = ((), (), s32[]{:S(2)}) async-start(), calls=%async_computation.7 | async-start | bytes 7864320 | tf_op jit(solution)/shard_map/reduce_scatter | solution.py:30
  755.9 19.4 %collective-permute-start.3 = (bf16[384,1024]{1,0:T(8,128)(2,1)S(1)}, bf16[384,1024]{1,0:T(8,128)(2,1)S(1)}, u32[]{:S(2)}, u32[]{:S(2)}) collective-permute-start(bf16[384,1024]{1,0:T(8,128)(2,1)S(1)} %add_convert_fusion.1), channel_id=1, source_target_pairs={{0,8},{8,16},{16,24},{24,0},{1,9},{9,17},{17,25},{25,1},{2,10},{10... | collective-permute-start | bytes 2359304 | tf_op jit(solution)/shard_map/ppermute | solution.py:15
  775.3 18.5 %collective-permute-start.4 = (bf16[384,1024]{1,0:T(8,128)(2,1)S(1)}, bf16[384,1024]{1,0:T(8,128)(2,1)S(1)}, u32[]{:S(2)}, u32[]{:S(2)}) collective-permute-start(bf16[384,1024]{1,0:T(8,128)(2,1)S(1)} %collective-permute-done.3), channel_id=1, source_target_pairs={{0,8},{8,16},{16,24},{24,0},{1,9},{9,17},{17,25},{25,1},{2,10},{10... | collective-permute-start | bytes 2359304 | tf_op jit(solution)/shard_map/ppermute | solution.py:15
  793.8 246.1 %collective-permute-start.5 = (bf16[384,1024]{1,0:T(8,128)(2,1)S(1)}, bf16[384,1024]{1,0:T(8,128)(2,1)S(1)}, u32[]{:S(2)}, u32[]{:S(2)}) collective-permute-start(bf16[384,1024]{1,0:T(8,128)(2,1)S(1)} %collective-permute-done.4), channel_id=1, source_target_pairs={{0,8},{8,16},{16,24},{24,0},{1,9},{9,17},{17,25},{25,1},{2,10},{10... | collective-permute-start | bytes 2359304 | tf_op jit(solution)/shard_map/ppermute | solution.py:15
  1360.3 123.8 %copy-start.3 = (f32[1024]{0:T(1024)S(1)}, f32[1024]{0:T(1024)}, u32[]{:S(2)}) copy-start(f32[1024]{0:T(1024)} %param.19) | copy-start | bytes 12292
  1360.3 123.8 %copy-start.4 = (f32[1024]{0:T(1024)S(1)}, f32[1024]{0:T(1024)}, u32[]{:S(2)}) copy-start(f32[1024]{0:T(1024)} %param.18) | copy-start | bytes 12292
Sparse Core Ops, SparseCore 0:
  9.2 299.7 all-gather.4
  310.9 297.0 all-gather.6
  629.8 110.7 reduce-scatter.2
  742.3 297.5 all-gather.8
  1041.7 297.0 all-gather.10
  1360.5 110.7 reduce-scatter.4
